TPU v7x, 32 devices: a whole 2x2x4 slice. The times are simulated.
32 devices in a mesh: grp: 1, fs: 2 (over x), tp: 16 (over z, y, core).
Axes of the slice: x: 2, y: 2, z: 4, core: 2. Of those that a mesh axis runs over, the one named last changes fastest.
Arguments:
- prompt_rows: bfloat16 [512, 2048], P(('grp', 'fs')), may hold values from -6 to 6
- gain_before: float32 [2048], P('fs'), may hold values from 0.1 to 1.9
- gate_before: float32 [2048, 5632], P('fs', 'tp'), may hold values from -0.125 to 0.125
- up_before: float32 [2048, 5632], P('fs', 'tp'), may hold values from -0.125 to 0.125
- down_before: float32 [5632, 2048], P('fs', 'tp'), may hold values from -0.3125 to 0.3125
- gain_after: float32 [2048], P('fs'), may hold values from 0.1 to 1.9
- gate_after: float32 [2048, 5632], P('fs', 'tp'), may hold values from -0.125 to 0.125
- up_after: float32 [2048, 5632], P('fs', 'tp'), may hold values from -0.125 to 0.125
- down_after: float32 [5632, 2048], P('fs', 'tp'), may hold values from -0.3125 to 0.3125
Outputs:
- mixed_rows: bfloat16 [512, 2048], P(('grp', 'fs'))
- served_gate_before: bfloat16 [2048, 5632], P('grp', 'tp')
- served_up_before: bfloat16 [2048, 5632], P('grp', 'tp')
- served_down_before: bfloat16 [5632, 2048], P(('grp', 'tp'))
- served_gate_after: bfloat16 [2048, 5632], P('grp', 'tp')
- served_up_after: bfloat16 [2048, 5632], P('grp', 'tp')
- served_down_after: bfloat16 [5632, 2048], P(('grp', 'tp'))
All inputs are finite; a program needn't handle non-finite values.
Results may differ from a plain program's by a relative error of at most 0.03.
Values may be sent and summed in bfloat16 or wider, within the bound.
No kernel may reach another device: no remote copies, remote signals or barrier semaphores. Data moves between devices by JAX's collectives and lax.ppermute only.
A program may use at most 64 MiB of HBM per device.

v0:
```python
import jax
import jax.numpy as jnp
from jax import lax
from jax.sharding import PartitionSpec as P

EPS = 1e-06


def serve_weights(gain, gate_w, up_w, down_w):
    gate_half = (gain[:, None] * gate_w).astype(jnp.bfloat16)
    up_half = (gain[:, None] * up_w).astype(jnp.bfloat16)
    down_half = down_w.astype(jnp.bfloat16)
    gate_whole, up_whole = (
        lax.all_gather(gate_half, "fs", axis=0, tiled=True),
        lax.all_gather(up_half, "fs", axis=0, tiled=True),
    )
    tall_block = lax.all_gather(down_half, "fs", axis=0, tiled=True)
    down_whole = lax.all_to_all(tall_block, "tp", split_axis=0, concat_axis=1, tiled=True)
    return (gate_whole, up_whole, down_whole)


def half_step(row_block, gate_w, up_w, down_w):
    values = row_block.astype(jnp.float32)
    normed = (values * lax.rsqrt(jnp.mean(values * values, axis=-1, keepdims=True) + EPS)).astype(
        jnp.bfloat16
    )
    gate_pre = jnp.dot(normed, gate_w, preferred_element_type=jnp.float32)
    up_pre = jnp.dot(normed, up_w, preferred_element_type=jnp.float32)
    hidden = (jax.nn.silu(gate_pre) * up_pre).astype(jnp.bfloat16)
    total = lax.psum(
        jnp.dot(hidden, down_w, preferred_element_type=jnp.float32).astype(jnp.bfloat16), "tp"
    ).astype(jnp.float32)
    return (values + 0.5 * total).astype(jnp.bfloat16)


def body(
    prompt_rows,
    gain_before,
    gate_before,
    up_before,
    down_before,
    gain_after,
    gate_after,
    up_after,
    down_after,
):
    gate_one, up_one, down_one = serve_weights(gain_before, gate_before, up_before, down_before)
    gate_two, up_two, down_two = serve_weights(gain_after, gate_after, up_after, down_after)
    middle = half_step(prompt_rows, gate_one, up_one, down_one)
    mixed = half_step(middle, gate_two, up_two, down_two)
    return (mixed, gate_one, up_one, down_one, gate_two, up_two, down_two)


def solution(mesh):
    placed = (
        P(("grp", "fs"), None),
        P("fs"),
        P("fs", "tp"),
        P("fs", "tp"),
        P("fs", "tp"),
        P("fs"),
        P("fs", "tp"),
        P("fs", "tp"),
        P("fs", "tp"),
    )
    return jax.shard_map(
        body,
        mesh=mesh,
        in_specs=placed,
        out_specs=(
            P(("grp", "fs"), None),
            P("grp", "tp"),
            P("grp", "tp"),
            P(("grp", "tp"), None),
            P("grp", "tp"),
            P("grp", "tp"),
            P(("grp", "tp"), None),
        ),
        check_vma=False,
    )
```

profile of v0, /device:TPU:0, one launch (start us, length us, event | category | flops | bytes accessed | tf_op | source)
XLA Modules:
  0.0 390.6 jit_solution(4047119397556258142)
XLA Ops:
  7.2 2.4 convert_element_type.59
  9.8 2.2 multiply_convert_fusion.3
  12.0 26.6 %all-gather.11.cloned.1.call-done = bf16[5632,128]{1,0:T(8,128)(2,1)} async-done(((bf16[2816,128]{1,0:T(8,128)(2,1)}), bf16[5632,128]{1,0:T(8,128)(2,1)}) %all-gather.11.cloned.1.call-update) | async-done | bytes 1441808 | tf_op jit(solution)/shard_map/all_gather | solution.py:17
  38.6 5.6 %all-to-all-start = ((bf16[16,352,128]{2,1,0:T(8,128)(2,1)}), bf16[16,352,128]{2,1,0:T(8,128)(2,1)S(1)}, u32[]{:S(2)}, u32[]{:S(2)}) async-start(bf16[16,352,128]{2,1,0:T(8,128)(2,1)} %bitcast.21), calls=%async_computation | async-start | bytes 2883584 | tf_op jit(solution)/shard_map/all_to_all | solution.py:18
  44.3 2.4 convert_element_type.68
  46.7 0.5 all-gather.9.cloned.1.call-update
  47.2 0.3 fusion
  47.5 18.9 %all-gather.7.cloned.1.call-done = bf16[2048,352]{0,1:T(8,128)(2,1)} async-done(((bf16[1024,352]{0,1:T(8,128)(2,1)}), bf16[2048,352]{0,1:T(8,128)(2,1)}) %all-gather.7.cloned.1.call-update) | async-done | bytes 1441808 | tf_op jit(solution)/shard_map/all_gather | solution.py:14
  66.4 2.0 fusion.14
  68.5 25.8 %all-gather.17.cloned.1.call-done = bf16[5632,128]{1,0:T(8,128)(2,1)} async-done(((bf16[2816,128]{1,0:T(8,128)(2,1)}), bf16[5632,128]{1,0:T(8,128)(2,1)}) %all-gather.17.cloned.1.call-update) | async-done | bytes 1441808 | tf_op jit(solution)/shard_map/all_gather | solution.py:17
  94.3 5.6 %all-to-all-start.1 = ((bf16[16,352,128]{2,1,0:T(8,128)(2,1)}), bf16[16,352,128]{2,1,0:T(8,128)(2,1)S(1)}, u32[]{:S(2)}, u32[]{:S(2)}) async-start(bf16[16,352,128]{2,1,0:T(8,128)(2,1)} %bitcast.20), calls=%async_computation.1 | async-start | bytes 2883584 | tf_op jit(solution)/shard_map/all_to_all | solution.py:18
  100.0 1.3 copy_bitcast_fusion.1
  101.3 20.7 %all-gather.9.cloned.1.call-done = bf16[2048,352]{0,1:T(8,128)(2,1)} async-done(((bf16[1024,352]{0,1:T(8,128)(2,1)}), bf16[2048,352]{0,1:T(8,128)(2,1)}) %all-gather.9.cloned.1.call-update) | async-done | bytes 1441808 | tf_op jit(solution)/shard_map/all_gather | solution.py:15
  122.0 5.3 %convolution_convert_fusion.1 = bf16[256,2048]{1,0:T(8,128)(2,1)} fusion(bf16[352,2048]{1,0:T(8,128)(2,1)} %copy_bitcast_fusion.1, bf16[2048,352]{0,1:T(8,128)(2,1)} %all-gather.9.cloned.1.call-done, bf16[256,2048]{1,0:T(8,128)(2,1)} %param.9, f32[256]{0:T(256)S(1)} %add_rsqrt_fusion.1, f32[256,352]{0,1:T(8,128)S(1)} %fusion.14), kind=kOutput, calls=%fused_computation.7 | convolution fusion | flops 740835328 | bytes 5342208 | tf_op jit(solution)/shard_map/dot_general | solution.py:31
  127.4 2.8 multiply_convert_fusion.1
  130.3 0.7 all-gather.15.cloned.1.call-update
  131.1 1.3 copy_bitcast_fusion
  132.4 89.0 %all-reduce.3.cloned.1.call-done = bf16[256,2048]{1,0:T(8,128)(2,1)} async-done(((bf16[256,2048]{1,0:T(8,128)(2,1)}), bf16[256,2048]{1,0:T(8,128)(2,1)}) %all-reduce.3.cloned.1.call-update) | async-done | bytes 1048592 | tf_op jit(solution)/shard_map/psum | solution.py:30
  221.3 1.8 fusion.3
  223.2 25.0 %all-gather.13.cloned.1.call-done = bf16[2048,352]{0,1:T(8,128)(2,1)} async-done(((bf16[1024,352]{0,1:T(8,128)(2,1)}), bf16[2048,352]{0,1:T(8,128)(2,1)}) %all-gather.13.cloned.1.call-update) | async-done | bytes 1441808 | tf_op jit(solution)/shard_map/all_gather | solution.py:14
  248.1 2.1 fusion.10
  250.3 25.7 %all-gather.15.cloned.1.call-done = bf16[2048,352]{0,1:T(8,128)(2,1)} async-done(((bf16[1024,352]{0,1:T(8,128)(2,1)}), bf16[2048,352]{0,1:T(8,128)(2,1)}) %all-gather.15.cloned.1.call-update) | async-done | bytes 1441808 | tf_op jit(solution)/shard_map/all_gather | solution.py:15
  276.0 4.4 %convolution_convert_fusion = bf16[256,2048]{1,0:T(8,128)(2,1)} fusion(bf16[352,2048]{1,0:T(8,128)(2,1)S(1)} %copy-done.9, bf16[2048,352]{0,1:T(8,128)(2,1)} %all-gather.15.cloned.1.call-done, bf16[256,2048]{1,0:T(8,128)(2,1)S(1)} %get-tuple-element.8, f32[256]{0:T(256)S(1)} %add_rsqrt_fusion, f32[256,352]{0,1:T(8,128)S(1)} %fusion.10), kind=kOutput, calls=%fused_computation.6 | convolution fusion | flops 740835328 | bytes 5342208 | tf_op jit(solution)/shard_map/dot_general | solution.py:31
  280.5 94.0 %all-reduce.5.cloned.1.call-done = bf16[256,2048]{1,0:T(8,128)(2,1)} async-done(((bf16[256,2048]{1,0:T(8,128)(2,1)}), bf16[256,2048]{1,0:T(8,128)(2,1)}) %all-reduce.5.cloned.1.call-update) | async-done | bytes 1048592 | tf_op jit(solution)/shard_map/psum | solution.py:30
  374.4 2.6 fusion.5
  377.0 1.1 copy.30
  378.1 0.8 copy-done.6
  378.9 1.1 copy.31
  380.0 0.8 copy-done.7
  380.8 1.1 copy.32
  381.9 0.8 copy-done.8
  382.7 1.1 copy.33
  (37 shorter events, 0.5 us)
Async XLA Ops:
  7.2 2.6 copy-start.2
  7.2 2.6 copy-start.3
  7.2 31.4 %all-gather.11.cloned.1.call-start = ((), (), s32[]{:S(2)}) async-start(), calls=%async_computation.4 | async-start | bytes 2162688 | tf_op jit(solution)/shard_map/all_gather | solution.py:17
  9.7 56.7 %all-gather.7.cloned.1.call-start = ((), (), s32[]{:S(2)}) async-start(), calls=%async_computation.2 | async-start | bytes 2162688 | tf_op jit(solution)/shard_map/all_gather | solution.py:14
  38.6 55.7 %all-to-all-start = ((bf16[16,352,128]{2,1,0:T(8,128)(2,1)}), bf16[16,352,128]{2,1,0:T(8,128)(2,1)S(1)}, u32[]{:S(2)}, u32[]{:S(2)}) async-start(bf16[16,352,128]{2,1,0:T(8,128)(2,1)} %bitcast.21), calls=%async_computation | async-start | bytes 2883584 | tf_op jit(solution)/shard_map/all_to_all | solution.py:18
  44.2 3.0 copy-start
  44.2 50.1 %all-gather.17.cloned.1.call-start = ((), (), s32[]{:S(2)}) async-start(), calls=%async_computation.8 | async-start | bytes 2162688 | tf_op jit(solution)/shard_map/all_gather | solution.py:17
  46.7 75.4 %all-gather.9.cloned.1.call-start = ((), (), s32[]{:S(2)}) async-start(), calls=%async_computation.3 | async-start | bytes 2162688 | tf_op jit(solution)/shard_map/all_gather | solution.py:15
  94.3 36.8 %all-to-all-start.1 = ((bf16[16,352,128]{2,1,0:T(8,128)(2,1)}), bf16[16,352,128]{2,1,0:T(8,128)(2,1)S(1)}, u32[]{:S(2)}, u32[]{:S(2)}) async-start(bf16[16,352,128]{2,1,0:T(8,128)(2,1)} %bitcast.20), calls=%async_computation.1 | async-start | bytes 2883584 | tf_op jit(solution)/shard_map/all_to_all | solution.py:18
  99.9 121.4 %all-reduce.3.cloned.1.call-start = ((), (), s32[]{:S(2)}) async-start(), calls=%async_computation.5 | async-start | bytes 2097152 | tf_op jit(solution)/shard_map/psum | solution.py:30
  101.3 26.1 %copy-start.10 = (f32[1024]{0:T(1024)S(1)}, f32[1024]{0:T(1024)}, u32[]{:S(2)}) copy-start(f32[1024]{0:T(1024)} %param.14) | copy-start | bytes 12292
  122.0 5.4 %copy-start.4 = (f32[1024,352]{0,1:T(8,128)S(1)}, f32[1024,352]{0,1:T(8,128)}, u32[]{:S(2)}) copy-start(f32[1024,352]{0,1:T(8,128)} %param.15) | copy-start | bytes 4325380
  127.3 120.8 %all-gather.13.cloned.1.call-start = ((), (), s32[]{:S(2)}) async-start(), calls=%async_computation.6 | async-start | bytes 2162688 | tf_op jit(solution)/shard_map/all_gather | solution.py:14
  130.3 145.7 %all-gather.15.cloned.1.call-start = ((), (), s32[]{:S(2)}) async-start(), calls=%async_computation.7 | async-start | bytes 2162688 | tf_op jit(solution)/shard_map/all_gather | solution.py:15
  131.0 90.3 %copy-start.1 = (bf16[256,2048]{1,0:T(8,128)(2,1)S(1)}, bf16[256,2048]{1,0:T(8,128)(2,1)}, u32[]{:S(2)}) copy-start(bf16[256,2048]{1,0:T(8,128)(2,1)} %param.9) | copy-start | bytes 3145732
  131.0 243.4 %all-reduce.5.cloned.1.call-start = ((), (), s32[]{:S(2)}) async-start(), calls=%async_computation.9 | async-start | bytes 2097152 | tf_op jit(solution)/shard_map/psum | solution.py:30
  248.1 27.9 %copy-start.9 = (bf16[352,2048]{1,0:T(8,128)(2,1)S(1)}, bf16[352,2048]{1,0:T(8,128)(2,1)}, u32[]{:S(2)}) copy-start(bf16[352,2048]{1,0:T(8,128)(2,1)} %copy_bitcast_fusion) | copy-start | bytes 4325380
  280.5 96.6 %copy-start.5 = (bf16[2048,352]{0,1:T(8,128)(2,1)S(1)}, bf16[2048,352]{0,1:T(8,128)(2,1)}, u32[]{:S(2)}) copy-start(bf16[2048,352]{0,1:T(8,128)(2,1)} %all-gather.7.cloned.1.call-done) | copy-start | bytes 4325380
  377.0 1.9 copy-start.6
  378.9 1.9 copy-start.7
  380.8 1.9 copy-start.8
Sparse Core Ops, SparseCore 0:
  10.1 28.4 all-gather.10
  40.7 25.6 all-gather.6
  68.6 25.6 all-gather.16
  96.3 25.6 all-gather.8
  127.5 93.8 all-reduce.2
  223.3 24.7 all-gather.12
  250.3 25.6 all-gather.14
  280.6 93.8 all-reduce.4
where the time goes:
time: 391 us
  waiting for transfers between devices  327 us (84%)
  other arithmetic  14.5 us (4%)
  between operations  14.3 us (4%)
  matrix products  13.9 us (4%)
  starting transfers between devices  11.6 us (3%)
  local copies, waits for them, and re-layouts  9.35 us (2%)
    psum x2, waiting for transfers between devices, half_step(): lax.psum(jnp.dot(hidden, down_w, preferred_element_type=jnp.float32).asty...  183 us
    all_gather x2, waiting for transfers between devices, serve_weights(): tall_block = lax.all_gather(down_half, 'fs', axis=0, tiled=True)  52.5 us
    all_gather x2, waiting for transfers between devices, serve_weights(): lax.all_gather(up_half, 'fs', axis=0, tiled=True)  46.5 us
    all_gather x2, waiting for transfers between devices, serve_weights(): lax.all_gather(gate_half, 'fs', axis=0, tiled=True)  43.9 us
    all_to_all x2, starting transfers between devices, serve_weights(): lax.all_to_all(tall_block, 'tp', split_axis=0, concat_axis=1, tiled=True)  11.2 us
    dot_general x2, matrix products, half_step(): jnp.dot(hidden, down_w, preferred_element_type=jnp.float32)  9.75 us
  transfers between devices with their start and end apart: 10, of which 8 were waited for; matrix products, arithmetic and copies ran while one was open for 5% of the time, Pallas kernels for 0%

commit v1 on v0

v1 whole, which is shorter than its diff:
```python
import jax
import jax.numpy as jnp
from jax import lax
from jax.sharding import PartitionSpec as P


EPS = 1e-06


def swap_fs(value, n_fs):
    return lax.ppermute(value, "fs", [(i, i ^ 1) for i in range(n_fs)])


def stack_fs(value, n_fs):
    if n_fs == 2:
        other = swap_fs(value, n_fs)
        first = lax.axis_index("fs") == 0
        return jnp.concatenate(
            [jnp.where(first, value, other), jnp.where(first, other, value)], axis=0
        )
    return lax.all_gather(value, "fs", axis=0, tiled=True)


def serve_down(down_w, n_fs, n_tp):
    down_half = down_w.astype(jnp.bfloat16)
    if n_fs != 2 or (down_w.shape[0] // n_tp) % 8:
        tall_block = lax.all_gather(down_half, "fs", axis=0, tiled=True)
        return lax.all_to_all(tall_block, "tp", split_axis=0, concat_axis=1, tiled=True)
    rows, width = down_w.shape[0] // n_tp, down_w.shape[1]
    parts = down_half.reshape(n_tp // 2, 2, rows, width)
    place = lax.axis_index("fs")
    keep = lax.dynamic_index_in_dim(parts, place, 1, keepdims=False)
    send = lax.dynamic_index_in_dim(parts, 1 - place, 1, keepdims=False)
    other = swap_fs(send, n_fs)
    first = place == 0
    tall = jnp.concatenate(
        [jnp.where(first, keep, other), jnp.where(first, other, keep)], axis=0
    )
    got = lax.all_to_all(tall, "tp", 0, 0, tiled=True)
    band = got.transpose(1, 0, 2).reshape(rows, n_tp * width)
    return stack_fs(band, n_fs)


def serve_weight(gain, weight, n_fs):
    half = (gain[:, None] * weight).astype(jnp.bfloat16)
    return stack_fs(half, n_fs)


def pair_swap(value, n_tp):
    return lax.ppermute(value, "tp", [(i, i ^ 1) for i in range(n_tp)])


def swap_places(value, n_tp, mask):
    return lax.ppermute(value, "tp", [(i, i ^ (2 * mask)) for i in range(n_tp)])


def scatter_sum(part, n_tp):
    rows, width = part.shape
    core, place = lax.axis_index("tp") % 2, lax.axis_index("tp") // 2
    places = n_tp // 2
    halves = part.reshape(2, rows // 2, width)
    keep = lax.dynamic_index_in_dim(halves, core, 0, keepdims=False)
    send = lax.dynamic_index_in_dim(halves, 1 - core, 0, keepdims=False)
    other = pair_swap(send, n_tp)
    both = keep.astype(jnp.float32) + other.astype(jnp.float32)
    bands = both.astype(jnp.bfloat16).reshape(places, rows // n_tp, width)
    got = [
        swap_places(lax.dynamic_index_in_dim(bands, place ^ mask, 0, keepdims=False), n_tp, mask)
        for mask in range(1, places)
    ]
    total = lax.dynamic_index_in_dim(bands, place, 0, keepdims=False).astype(jnp.float32)
    for piece in got:
        total = total + piece.astype(jnp.float32)
    return total


def my_band(rows_block, n_tp):
    rows = rows_block.shape[0] // n_tp
    index = lax.axis_index("tp")
    band = (index % 2) * (n_tp // 2) + index // 2
    return lax.dynamic_slice_in_dim(rows_block, band * rows, rows, axis=0)


def gather_bands(band, n_tp):
    place, places = lax.axis_index("tp") // 2, n_tp // 2
    got = [band] + [swap_places(band, n_tp, mask) for mask in range(1, places)]
    half = jnp.zeros((places,) + band.shape, band.dtype)
    for mask, piece in enumerate(got):
        half = lax.dynamic_update_index_in_dim(half, piece, place ^ mask, 0)
    half = half.reshape(-1, band.shape[1])
    other = pair_swap(half, n_tp)
    first = lax.axis_index("tp") % 2 == 0
    return jnp.concatenate([jnp.where(first, half, other), jnp.where(first, other, half)], axis=0)


def normalise(values):
    return (values * lax.rsqrt(jnp.mean(values * values, axis=-1, keepdims=True) + EPS)).astype(
        jnp.bfloat16
    )


def part_of(normed, gate_w, up_w, down_w):
    gate_pre = jnp.dot(normed, gate_w, preferred_element_type=jnp.float32)
    up_pre = jnp.dot(normed, up_w, preferred_element_type=jnp.float32)
    hidden = (jax.nn.silu(gate_pre) * up_pre).astype(jnp.bfloat16)
    return jnp.dot(hidden, down_w, preferred_element_type=jnp.float32).astype(jnp.bfloat16)


def make_body(n_fs, n_tp):
    def body(
        prompt_rows,
        gain_before,
        gate_before,
        up_before,
        down_before,
        gain_after,
        gate_after,
        up_after,
        down_after,
    ):
      one = (
          serve_weight(gain_before, gate_before, n_fs),
          serve_weight(gain_before, up_before, n_fs),
          serve_down(down_before, n_fs, n_tp),
      )
      two = (
          serve_weight(gain_after, gate_after, n_fs),
          serve_weight(gain_after, up_after, n_fs),
          serve_down(down_after, n_fs, n_tp),
      )
      normed = normalise(prompt_rows.astype(jnp.float32))
      band = my_band(prompt_rows, n_tp).astype(jnp.float32)
      total = scatter_sum(part_of(normed, *one), n_tp)
      middle = (band + 0.5 * total).astype(jnp.bfloat16).astype(jnp.float32)
      normed = gather_bands(normalise(middle), n_tp)
      total = scatter_sum(part_of(normed, *two), n_tp)
      mixed = gather_bands((middle + 0.5 * total).astype(jnp.bfloat16), n_tp)
      return (mixed,) + one + two

    return body


def solution(mesh):
    placed = (
        P(("grp", "fs"), None),
        P("fs"),
        P("fs", "tp"),
        P("fs", "tp"),
        P("fs", "tp"),
        P("fs"),
        P("fs", "tp"),
        P("fs", "tp"),
        P("fs", "tp"),
    )
    return jax.shard_map(
        make_body(mesh.shape["fs"], mesh.shape["tp"]),
        mesh=mesh,
        in_specs=placed,
        out_specs=(
            P(("grp", "fs"), None),
            P("grp", "tp"),
            P("grp", "tp"),
            P(("grp", "tp"), None),
            P("grp", "tp"),
            P("grp", "tp"),
            P(("grp", "tp"), None),
        ),
        check_vma=False,
    )
```

time: 391 us -> 199 us (0.51)
  waiting for transfers between devices: 327 us -> 80.2 us
  starting transfers between devices: 11.6 us -> 71.7 us
  between operations: 14.3 us -> 1.19 us
  other arithmetic: 14.5 us -> 26 us
    psum x2 -> x0, waiting for transfers between devices: 183 us -> none  [half_step(): lax.psum(jnp.dot(hidden, down_w, preferred_element_type=jnp.float32).asty...]
    all_gather x6 -> x0, waiting for transfers between devices: 143 us -> none  [the longest x2 52.5 us: serve_weights(): tall_block = lax.all_gather(down_half, 'fs', axis=0, tiled=True)]
    ppermute x0 -> x40, waiting for transfers between devices: none -> 80.2 us  [the longest x8 56 us: swap_fs(): return lax.ppermute(value, 'fs', [(i, i ^ 1) for i in range(n_fs)])]
    ppermute x0 -> x40, starting transfers between devices: none -> 59.3 us  [the longest x28 46 us: swap_places(): return lax.ppermute(value, 'tp', [(i, i ^ 2 * mask) for i in range(n_tp)])]
    select_n x0 -> x10, other arithmetic: none -> 10.3 us  [the longest x6 7.87 us: stack_fs(): jnp.where(first, value, other)]
    concatenate x0 -> x9, other arithmetic: none -> 9.02 us  [the longest x6 6.1 us: stack_fs(): jnp.concatenate([jnp.where(first, value, other), jnp.where(first, other,...]
    convert_element_type x5 -> x6, other arithmetic: 12.4 us -> 4.84 us  [the longest x2 2.97 us: serve_weight(): half = (gain[:, None] * weight).astype(jnp.bfloat16)]
  transfers between devices with their start and end apart: 10 -> 42, of which waited for: 8 -> 18; matrix products, arithmetic and copies ran while one was open for 5% -> 16% of each run, Pallas kernels for 0% -> 0%
where the time goes in v1:
time: 199 us; the launch traced here: 198 us
  waiting for transfers between devices  80.2 us (40%)
  starting transfers between devices  71.7 us (36%)
  other arithmetic  26 us (13%)
  matrix products  11.6 us (6%)
  local copies, waits for them, and re-layouts  7.11 us (4%)
    ppermute x8, waiting for transfers between devices, swap_fs(): return lax.ppermute(value, 'fs', [(i, i ^ 1) for i in range(n_fs)])  56 us
    ppermute x28, starting transfers between devices, swap_places(): return lax.ppermute(value, 'tp', [(i, i ^ 2 * mask) for i in range(n_tp)])  46 us
    ppermute x28, waiting for transfers between devices, swap_places(): return lax.ppermute(value, 'tp', [(i, i ^ 2 * mask) for i in range(n_tp)])  20.3 us
    all_to_all x2, starting transfers between devices, serve_down(): got = lax.all_to_all(tall, 'tp', 0, 0, tiled=True)  12.4 us
    ppermute x8, starting transfers between devices, swap_fs(): return lax.ppermute(value, 'fs', [(i, i ^ 1) for i in range(n_fs)])  12.3 us
    dot_general x2, matrix products, part_of(): jnp.dot(hidden, down_w, preferred_element_type=jnp.float32)  8.86 us
    select_n x6, other arithmetic, stack_fs(): jnp.where(first, value, other)  7.87 us
    concatenate x6, other arithmetic, stack_fs(): jnp.concatenate([jnp.where(first, value, other), jnp.where(first, other,...  6.1 us
  transfers between devices with their start and end apart: 42, of which 18 were waited for; matrix products, arithmetic and copies ran while one was open for 16% of the time, Pallas kernels for 0%

profile of v1, /device:TPU:0, one launch (start us, length us, event | category | flops | bytes accessed | tf_op | source)
XLA Modules:
  0.0 197.8 jit_solution(4730205806882826499)
XLA Ops:
  3.0 3.0 %collective-permute-start.2 = (bf16[8,176,128]{2,1,0:T(8,128)(2,1)}, bf16[8,176,128]{2,1,0:T(8,128)(2,1)}, u32[]{:S(2)}, u32[]{:S(2)}) collective-permute-start(bf16[8,176,128]{2,1,0:T(8,128)(2,1)} %dynamic-slice_bitcast_fusion.3), channel_id=1, source_target_pairs={{0,16},{16,0},{1,17},{17,1},{2,18},{18,2},{3,19},{19,3},{4,20},{20... | collective-permute-start | bytes 1081352 | tf_op jit(solution)/shard_map/ppermute | solution.py:11
  6.0 2.6 %multiply_convert_fusion.3 = (bf16[1024,352]{0,1:T(8,128)(2,1)S(1)}, bf16[1024,352]{0,1:T(8,128)(2,1)}) fusion(f32[1024,352]{0,1:T(8,128)S(1)} %copy-done.5, f32[1024]{0:T(1024)S(1)} %copy-done.17, f32[1024,352]{0,1:T(8,128)} %param.12), kind=kLoop, calls=%fused_computation.15 | loop fusion | flops 1441792 | bytes 4329472 | tf_op jit(solution)/shard_map/convert_element_type | solution.py:45
  8.7 1.8 collective-permute-start
  12.2 1.9 collective-permute-start.22
  15.5 2.0 %collective-permute-start.20 = (bf16[1024,352]{0,1:T(8,128)(2,1)S(1)}, bf16[1024,352]{0,1:T(8,128)(2,1)}, u32[]{:S(2)}, u32[]{:S(2)}) collective-permute-start(bf16[1024,352]{0,1:T(8,128)(2,1)S(1)} %get-tuple-element.47), channel_id=1, source_target_pairs={{0,16},{16,0},{1,17},{17,1},{2,18},{18,2},{3,19},{19,3},{4,20},{20... | collective-permute-start | bytes 2162696 | tf_op jit(solution)/shard_map/ppermute | solution.py:11
  19.5 5.9 %all-to-all-start = ((bf16[16,176,128]{2,1,0:T(8,128)(2,1)}), bf16[16,176,128]{2,1,0:T(8,128)(2,1)S(1)}, u32[]{:S(2)}, u32[]{:S(2)}) async-start(bf16[16,176,128]{2,1,0:T(8,128)(2,1)} %pad_maximum_fusion.8), calls=%async_computation | async-start | bytes 1441792 | tf_op jit(solution)/shard_map/all_to_all | solution.py:39
  27.0 42.5 %collective-permute-done.22 = bf16[8,176,128]{2,1,0:T(8,128)(2,1)} collective-permute-done((bf16[8,176,128]{2,1,0:T(8,128)(2,1)S(1)}, bf16[8,176,128]{2,1,0:T(8,128)(2,1)}, u32[]{:S(2)}, u32[]{:S(2)}) %collective-permute-start.22) | collective-permute-done | bytes 360480 | tf_op jit(solution)/shard_map/ppermute | solution.py:11
  71.7 2.5 %broadcast_select_fusion.9 = (bf16[1024,352]{0,1:T(8,128)(2,1)}, bf16[1024,352]{0,1:T(8,128)(2,1)}) fusion(bf16[1024,352]{0,1:T(8,128)(2,1)} %get-tuple-element.50, bf16[1024,352]{0,1:T(8,128)(2,1)} %collective-permute-done.1, pred[]{:T(512)S(6)} %eq.11), kind=kLoop, calls=%fused_computation.35 | loop fusion | flops 720896 | bytes 2883585 | tf_op jit(solution)/shard_map/jit(_where)/select_n | solution.py:19
  74.2 2.3 %broadcast_select_fusion.11 = (bf16[1024,352]{0,1:T(8,128)(2,1)}, bf16[1024,352]{0,1:T(8,128)(2,1)}) fusion(bf16[1024,352]{0,1:T(8,128)(2,1)S(1)} %get-tuple-element.49, bf16[1024,352]{0,1:T(8,128)(2,1)} %collective-permute-done, pred[]{:T(512)S(6)} %eq.11), kind=kLoop, calls=%fused_computation.37 | loop fusion | flops 720896 | bytes 2883585 | tf_op jit(solution)/shard_map/jit(_where)/select_n | solution.py:19
  76.5 6.5 %all-to-all-start.1 = ((bf16[16,176,128]{2,1,0:T(8,128)(2,1)}), bf16[16,176,128]{2,1,0:T(8,128)(2,1)S(1)}, u32[]{:S(2)}, u32[]{:S(2)}) async-start(bf16[16,176,128]{2,1,0:T(8,128)(2,1)} %pad_maximum_fusion.9), calls=%async_computation.1 | async-start | bytes 1441792 | tf_op jit(solution)/shard_map/all_to_all | solution.py:39
  89.6 12.0 %collective-permute-done.3 = bf16[176,2048]{1,0:T(8,128)(2,1)S(1)} collective-permute-done((bf16[176,2048]{1,0:T(8,128)(2,1)S(1)}, bf16[176,2048]{1,0:T(8,128)(2,1)S(1)}, u32[]{:S(2)}, u32[]{:S(2)}) %collective-permute-start.3) | collective-permute-done | bytes 720928 | tf_op jit(solution)/shard_map/ppermute | solution.py:11
  103.6 5.0 %convolution_convert_fusion.1 = bf16[256,2048]{1,0:T(8,128)(2,1)} fusion(bf16[352,2048]{1,0:T(8,128)(2,1)} %pad_maximum_fusion.2, f32[256,352]{0,1:T(8,128)} %fusion.6, bf16[2048,352]{0,1:T(8,128)(2,1)} %pad_maximum_fusion, bf16[256,2048]{1,0:T(8,128)(2,1)S(1)} %copy-done.13, f32[256]{0:T(256)S(1)} %add_rsqrt_fusion), kind=kOutput, calls=%fused_computation.3 | convolution fusion | flops 740835328 | bytes 5342208 | tf_op jit(solution)/shard_map/dot_general | solution.py:106
  112.6 3.5 %collective-permute-start.10 = (bf16[16,2048]{1,0:T(8,128)(2,1)S(1)}, bf16[16,2048]{1,0:T(8,128)(2,1)S(1)}, u32[]{:S(2)}, u32[]{:S(2)}) collective-permute-start(bf16[16,2048]{1,0:T(8,128)(2,1)S(1)} %get-tuple-element.42), channel_id=1, source_target_pairs={{0,12},{1,13},{2,14},{3,15},{4,8},{5,9},{6,10},{7,11},{8,4},{9,5},... | collective-permute-start | bytes 196616 | tf_op jit(solution)/shard_map/ppermute | solution.py:54
  119.2 3.1 %collective-permute-start.7 = (bf16[16,2048]{1,0:T(8,128)(2,1)S(1)}, bf16[16,2048]{1,0:T(8,128)(2,1)S(1)}, u32[]{:S(2)}, u32[]{:S(2)}) collective-permute-start(bf16[16,2048]{1,0:T(8,128)(2,1)S(1)} %get-tuple-element.45), channel_id=1, source_target_pairs={{0,6},{1,7},{2,4},{3,5},{4,2},{5,3},{6,0},{7,1},{8,14},{9,15},{10,... | collective-permute-start | bytes 196616 | tf_op jit(solution)/shard_map/ppermute | solution.py:54
  122.3 1.8 collective-permute-start.8
  126.7 3.0 %collective-permute-done.8 = bf16[16,2048]{1,0:T(8,128)(2,1)S(1)} collective-permute-done((bf16[16,2048]{1,0:T(8,128)(2,1)S(1)}, bf16[16,2048]{1,0:T(8,128)(2,1)S(1)}, u32[]{:S(2)}, u32[]{:S(2)}) %collective-permute-start.8) | collective-permute-done | bytes 65568 | tf_op jit(solution)/shard_map/ppermute | solution.py:54
  131.0 1.9 collective-permute-start.12
  137.7 2.8 %collective-permute-start.16 = (bf16[16,2048]{1,0:T(8,128)(2,1)S(1)}, bf16[16,2048]{1,0:T(8,128)(2,1)S(1)}, u32[]{:S(2)}, u32[]{:S(2)}) collective-permute-start(bf16[16,2048]{1,0:T(8,128)(2,1)S(1)} %get-tuple-element.10), channel_id=1, source_target_pairs={{0,10},{1,11},{2,8},{3,9},{4,14},{5,15},{6,12},{7,13},{8,2},{9,3},... | collective-permute-start | bytes 196616 | tf_op jit(solution)/shard_map/ppermute | solution.py:54
  140.5 2.6 %collective-permute-start.17 = (bf16[16,2048]{1,0:T(8,128)(2,1)S(1)}, bf16[16,2048]{1,0:T(8,128)(2,1)S(1)}, u32[]{:S(2)}, u32[]{:S(2)}) collective-permute-start(bf16[16,2048]{1,0:T(8,128)(2,1)S(1)} %get-tuple-element.10), channel_id=1, source_target_pairs={{0,12},{1,13},{2,14},{3,15},{4,8},{5,9},{6,10},{7,11},{8,4},{9,5},... | collective-permute-start | bytes 196616 | tf_op jit(solution)/shard_map/ppermute | solution.py:54
  144.2 4.4 %collective-permute-done.16 = bf16[16,2048]{1,0:T(8,128)(2,1)S(1)} collective-permute-done((bf16[16,2048]{1,0:T(8,128)(2,1)S(1)}, bf16[16,2048]{1,0:T(8,128)(2,1)S(1)}, u32[]{:S(2)}, u32[]{:S(2)}) %collective-permute-start.16) | collective-permute-done | bytes 65568 | tf_op jit(solution)/shard_map/ppermute | solution.py:54
  154.6 3.9 %convolution_convert_fusion = bf16[256,2048]{1,0:T(8,128)(2,1)S(1)} fusion(bf16[352,2048]{1,0:T(8,128)(2,1)} %pad_maximum_fusion.5, f32[256,352]{0,1:T(8,128)} %fusion.4, bf16[2048,352]{0,1:T(8,128)(2,1)S(1)} %copy-done.11, bf16[128,2048]{1,0:T(8,128)(2,1)} %copy-done.16, bf16[128,2048]{1,0:T(8,128)(2,1)} %copy-done.15), kind=kOutput, calls=%fused_computation.2 | convolution fusion | flops 741359616 | bytes 5341184 | tf_op jit(solution)/shard_map/dot_general | solution.py:106
  164.6 1.9 collective-permute-start.28
  167.5 2.4 %collective-permute-start.30 = (bf16[16,2048]{1,0:T(8,128)(2,1)S(1)}, bf16[16,2048]{1,0:T(8,128)(2,1)S(1)}, u32[]{:S(2)}, u32[]{:S(2)}) collective-permute-start(bf16[16,2048]{1,0:T(8,128)(2,1)S(1)} %get-tuple-element.35), channel_id=1, source_target_pairs={{0,12},{1,13},{2,14},{3,15},{4,8},{5,9},{6,10},{7,11},{8,4},{9,5},... | collective-permute-start | bytes 196616 | tf_op jit(solution)/shard_map/ppermute | solution.py:54
  169.9 2.4 %collective-permute-start.31 = (bf16[16,2048]{1,0:T(8,128)(2,1)S(1)}, bf16[16,2048]{1,0:T(8,128)(2,1)S(1)}, u32[]{:S(2)}, u32[]{:S(2)}) collective-permute-start(bf16[16,2048]{1,0:T(8,128)(2,1)S(1)} %get-tuple-element.34), channel_id=1, source_target_pairs={{0,14},{1,15},{2,12},{3,13},{4,10},{5,11},{6,8},{7,9},{8,6},{9,7},... | collective-permute-start | bytes 196616 | tf_op jit(solution)/shard_map/ppermute | solution.py:54
  173.8 2.3 %collective-permute-done.29 = bf16[16,2048]{1,0:T(8,128)(2,1)S(1)} collective-permute-done((bf16[16,2048]{1,0:T(8,128)(2,1)S(1)}, bf16[16,2048]{1,0:T(8,128)(2,1)S(1)}, u32[]{:S(2)}, u32[]{:S(2)}) %collective-permute-start.29) | collective-permute-done | bytes 65568 | tf_op jit(solution)/shard_map/ppermute | solution.py:54
  177.1 1.8 collective-permute-start.32
  178.9 2.2 %collective-permute-start.33 = (bf16[16,2048]{1,0:T(8,128)(2,1)S(1)}, bf16[16,2048]{1,0:T(8,128)(2,1)S(1)}, u32[]{:S(2)}, u32[]{:S(2)}) collective-permute-start(bf16[16,2048]{1,0:T(8,128)(2,1)S(1)} %get-tuple-element.8), channel_id=1, source_target_pairs={{0,4},{1,5},{2,6},{3,7},{4,0},{5,1},{6,2},{7,3},{8,12},{9,13},{10,... | collective-permute-start | bytes 196616 | tf_op jit(solution)/shard_map/ppermute | solution.py:54
  181.7 2.6 %collective-permute-start.35 = (bf16[16,2048]{1,0:T(8,128)(2,1)S(1)}, bf16[16,2048]{1,0:T(8,128)(2,1)S(1)}, u32[]{:S(2)}, u32[]{:S(2)}) collective-permute-start(bf16[16,2048]{1,0:T(8,128)(2,1)S(1)} %get-tuple-element.8), channel_id=1, source_target_pairs={{0,8},{1,9},{2,10},{3,11},{4,12},{5,13},{6,14},{7,15},{8,0},{9,1},... | collective-permute-start | bytes 196616 | tf_op jit(solution)/shard_map/ppermute | solution.py:54
  185.1 2.4 %collective-permute-start.37 = (bf16[16,2048]{1,0:T(8,128)(2,1)S(1)}, bf16[16,2048]{1,0:T(8,128)(2,1)S(1)}, u32[]{:S(2)}, u32[]{:S(2)}) collective-permute-start(bf16[16,2048]{1,0:T(8,128)(2,1)S(1)} %get-tuple-element.8), channel_id=1, source_target_pairs={{0,12},{1,13},{2,14},{3,15},{4,8},{5,9},{6,10},{7,11},{8,4},{9,5},... | collective-permute-start | bytes 196616 | tf_op jit(solution)/shard_map/ppermute | solution.py:54
  187.5 2.0 collective-permute-start.38
  189.5 2.6 %collective-permute-done.35 = bf16[16,2048]{1,0:T(8,128)(2,1)S(1)} collective-permute-done((bf16[16,2048]{1,0:T(8,128)(2,1)S(1)}, bf16[16,2048]{1,0:T(8,128)(2,1)S(1)}, u32[]{:S(2)}, u32[]{:S(2)}) %collective-permute-start.35) | collective-permute-done | bytes 65568 | tf_op jit(solution)/shard_map/ppermute | solution.py:54
  194.7 1.9 collective-permute-done.39
  (149 shorter events, 57.2 us)
Async XLA Ops:
  3.0 12.5 %collective-permute-start.2 = (bf16[8,176,128]{2,1,0:T(8,128)(2,1)}, bf16[8,176,128]{2,1,0:T(8,128)(2,1)}, u32[]{:S(2)}, u32[]{:S(2)}) collective-permute-start(bf16[8,176,128]{2,1,0:T(8,128)(2,1)} %dynamic-slice_bitcast_fusion.3), channel_id=1, source_target_pairs={{0,16},{16,0},{1,17},{17,1},{2,18},{18,2},{3,19},{19,3},{4,20},{20... | collective-permute-start | bytes 1081352 | tf_op jit(solution)/shard_map/ppermute | solution.py:11
  8.5 63.1 %collective-permute-start.1 = (bf16[1024,352]{0,1:T(8,128)(2,1)}, bf16[1024,352]{0,1:T(8,128)(2,1)}, u32[]{:S(2)}, u32[]{:S(2)}) collective-permute-start(bf16[1024,352]{0,1:T(8,128)(2,1)} %get-tuple-element.50), channel_id=1, source_target_pairs={{0,16},{16,0},{1,17},{17,1},{2,18},{18,2},{3,19},{19,3},{4,20},{20... | collective-permute-start | bytes 2162696 | tf_op jit(solution)/shard_map/ppermute | solution.py:11
  8.7 65.5 %collective-permute-start = (bf16[1024,352]{0,1:T(8,128)(2,1)S(1)}, bf16[1024,352]{0,1:T(8,128)(2,1)}, u32[]{:S(2)}, u32[]{:S(2)}) collective-permute-start(bf16[1024,352]{0,1:T(8,128)(2,1)S(1)} %get-tuple-element.49), channel_id=1, source_target_pairs={{0,16},{16,0},{1,17},{17,1},{2,18},{18,2},{3,19},{19,3},{4,20},{20... | collective-permute-start | bytes 2162696 | tf_op jit(solution)/shard_map/ppermute | solution.py:11
  11.0 98.8 %collective-permute-start.21 = (bf16[1024,352]{0,1:T(8,128)(2,1)S(1)}, bf16[1024,352]{0,1:T(8,128)(2,1)}, u32[]{:S(2)}, u32[]{:S(2)}) collective-permute-start(bf16[1024,352]{0,1:T(8,128)(2,1)S(1)} %get-tuple-element.48), channel_id=1, source_target_pairs={{0,16},{16,0},{1,17},{17,1},{2,18},{18,2},{3,19},{19,3},{4,20},{20... | collective-permute-start | bytes 2162696 | tf_op jit(solution)/shard_map/ppermute | solution.py:11
  12.2 57.4 %collective-permute-start.22 = (bf16[8,176,128]{2,1,0:T(8,128)(2,1)S(1)}, bf16[8,176,128]{2,1,0:T(8,128)(2,1)}, u32[]{:S(2)}, u32[]{:S(2)}) collective-permute-start(bf16[8,176,128]{2,1,0:T(8,128)(2,1)S(1)} %dynamic-slice_bitcast_fusion.2), channel_id=1, source_target_pairs={{0,16},{16,0},{1,17},{17,1},{2,18},{18,2},{3,19},{19,3},{4,20},{20... | collective-permute-start | bytes 1081352 | tf_op jit(solution)/shard_map/ppermute | solution.py:11
  15.5 95.5 %collective-permute-start.20 = (bf16[1024,352]{0,1:T(8,128)(2,1)S(1)}, bf16[1024,352]{0,1:T(8,128)(2,1)}, u32[]{:S(2)}, u32[]{:S(2)}) collective-permute-start(bf16[1024,352]{0,1:T(8,128)(2,1)S(1)} %get-tuple-element.47), channel_id=1, source_target_pairs={{0,16},{16,0},{1,17},{17,1},{2,18},{18,2},{3,19},{19,3},{4,20},{20... | collective-permute-start | bytes 2162696 | tf_op jit(solution)/shard_map/ppermute | solution.py:11
  19.5 57.0 %all-to-all-start = ((bf16[16,176,128]{2,1,0:T(8,128)(2,1)}), bf16[16,176,128]{2,1,0:T(8,128)(2,1)S(1)}, u32[]{:S(2)}, u32[]{:S(2)}) async-start(bf16[16,176,128]{2,1,0:T(8,128)(2,1)} %pad_maximum_fusion.8), calls=%async_computation | async-start | bytes 1441792 | tf_op jit(solution)/shard_map/all_to_all | solution.py:39
  76.5 56.5 %all-to-all-start.1 = ((bf16[16,176,128]{2,1,0:T(8,128)(2,1)}), bf16[16,176,128]{2,1,0:T(8,128)(2,1)S(1)}, u32[]{:S(2)}, u32[]{:S(2)}) async-start(bf16[16,176,128]{2,1,0:T(8,128)(2,1)} %pad_maximum_fusion.9), calls=%async_computation.1 | async-start | bytes 1441792 | tf_op jit(solution)/shard_map/all_to_all | solution.py:39
  83.1 18.5 %collective-permute-start.3 = (bf16[176,2048]{1,0:T(8,128)(2,1)S(1)}, bf16[176,2048]{1,0:T(8,128)(2,1)S(1)}, u32[]{:S(2)}, u32[]{:S(2)}) collective-permute-start(bf16[176,2048]{1,0:T(8,128)(2,1)S(1)} %copy_bitcast_fusion.1), channel_id=1, source_target_pairs={{0,16},{16,0},{1,17},{17,1},{2,18},{18,2},{3,19},{19,3},{4,20},{20... | collective-permute-start | bytes 2162696 | tf_op jit(solution)/shard_map/ppermute | solution.py:11
  112.6 9.6 %collective-permute-start.10 = (bf16[16,2048]{1,0:T(8,128)(2,1)S(1)}, bf16[16,2048]{1,0:T(8,128)(2,1)S(1)}, u32[]{:S(2)}, u32[]{:S(2)}) collective-permute-start(bf16[16,2048]{1,0:T(8,128)(2,1)S(1)} %get-tuple-element.42), channel_id=1, source_target_pairs={{0,12},{1,13},{2,14},{3,15},{4,8},{5,9},{6,10},{7,11},{8,4},{9,5},... | collective-permute-start | bytes 196616 | tf_op jit(solution)/shard_map/ppermute | solution.py:54
  116.1 8.0 %collective-permute-start.11 = (bf16[16,2048]{1,0:T(8,128)(2,1)S(1)}, bf16[16,2048]{1,0:T(8,128)(2,1)S(1)}, u32[]{:S(2)}, u32[]{:S(2)}) collective-permute-start(bf16[16,2048]{1,0:T(8,128)(2,1)S(1)} %get-tuple-element.41), channel_id=1, source_target_pairs={{0,14},{1,15},{2,12},{3,13},{4,10},{5,11},{6,8},{7,9},{8,6},{9,7},... | collective-permute-start | bytes 196616 | tf_op jit(solution)/shard_map/ppermute | solution.py:54
  118.8 7.5 %collective-permute-start.5 = (bf16[16,2048]{1,0:T(8,128)(2,1)S(1)}, bf16[16,2048]{1,0:T(8,128)(2,1)S(1)}, u32[]{:S(2)}, u32[]{:S(2)}) collective-permute-start(bf16[16,2048]{1,0:T(8,128)(2,1)S(1)} %get-tuple-element.40), channel_id=1, source_target_pairs={{0,2},{1,3},{2,0},{3,1},{4,6},{5,7},{6,4},{7,5},{8,10},{9,11},{10,... | collective-permute-start | bytes 196616 | tf_op jit(solution)/shard_map/ppermute | solution.py:54
  119.2 7.5 %collective-permute-start.7 = (bf16[16,2048]{1,0:T(8,128)(2,1)S(1)}, bf16[16,2048]{1,0:T(8,128)(2,1)S(1)}, u32[]{:S(2)}, u32[]{:S(2)}) collective-permute-start(bf16[16,2048]{1,0:T(8,128)(2,1)S(1)} %get-tuple-element.45), channel_id=1, source_target_pairs={{0,6},{1,7},{2,4},{3,5},{4,2},{5,3},{6,0},{7,1},{8,14},{9,15},{10,... | collective-permute-start | bytes 196616 | tf_op jit(solution)/shard_map/ppermute | solution.py:54
  122.3 7.4 %collective-permute-start.8 = (bf16[16,2048]{1,0:T(8,128)(2,1)S(1)}, bf16[16,2048]{1,0:T(8,128)(2,1)S(1)}, u32[]{:S(2)}, u32[]{:S(2)}) collective-permute-start(bf16[16,2048]{1,0:T(8,128)(2,1)S(1)} %get-tuple-element.44), channel_id=1, source_target_pairs={{0,8},{1,9},{2,10},{3,11},{4,12},{5,13},{6,14},{7,15},{8,0},{9,1},... | collective-permute-start | bytes 196616 | tf_op jit(solution)/shard_map/ppermute | solution.py:54
  133.1 17.2 %collective-permute-start.23 = (bf16[176,2048]{1,0:T(8,128)(2,1)S(1)}, bf16[176,2048]{1,0:T(8,128)(2,1)S(1)}, u32[]{:S(2)}, u32[]{:S(2)}) collective-permute-start(bf16[176,2048]{1,0:T(8,128)(2,1)S(1)} %copy_bitcast_fusion), channel_id=1, source_target_pairs={{0,16},{16,0},{1,17},{17,1},{2,18},{18,2},{3,19},{19,3},{4,20},{20... | collective-permute-start | bytes 2162696 | tf_op jit(solution)/shard_map/ppermute | solution.py:11
  134.9 8.2 %collective-permute-start.14 = (bf16[16,2048]{1,0:T(8,128)(2,1)S(1)}, bf16[16,2048]{1,0:T(8,128)(2,1)S(1)}, u32[]{:S(2)}, u32[]{:S(2)}) collective-permute-start(bf16[16,2048]{1,0:T(8,128)(2,1)S(1)} %get-tuple-element.10), channel_id=1, source_target_pairs={{0,6},{1,7},{2,4},{3,5},{4,2},{5,3},{6,0},{7,1},{8,14},{9,15},{10,... | collective-permute-start | bytes 196616 | tf_op jit(solution)/shard_map/ppermute | solution.py:54
  136.2 8.0 %collective-permute-start.15 = (bf16[16,2048]{1,0:T(8,128)(2,1)S(1)}, bf16[16,2048]{1,0:T(8,128)(2,1)S(1)}, u32[]{:S(2)}, u32[]{:S(2)}) collective-permute-start(bf16[16,2048]{1,0:T(8,128)(2,1)S(1)} %get-tuple-element.10), channel_id=1, source_target_pairs={{0,8},{1,9},{2,10},{3,11},{4,12},{5,13},{6,14},{7,15},{8,0},{9,1},... | collective-permute-start | bytes 196616 | tf_op jit(solution)/shard_map/ppermute | solution.py:54
  137.7 10.9 %collective-permute-start.16 = (bf16[16,2048]{1,0:T(8,128)(2,1)S(1)}, bf16[16,2048]{1,0:T(8,128)(2,1)S(1)}, u32[]{:S(2)}, u32[]{:S(2)}) collective-permute-start(bf16[16,2048]{1,0:T(8,128)(2,1)S(1)} %get-tuple-element.10), channel_id=1, source_target_pairs={{0,10},{1,11},{2,8},{3,9},{4,14},{5,15},{6,12},{7,13},{8,2},{9,3},... | collective-permute-start | bytes 196616 | tf_op jit(solution)/shard_map/ppermute | solution.py:54
  140.5 8.1 %collective-permute-start.17 = (bf16[16,2048]{1,0:T(8,128)(2,1)S(1)}, bf16[16,2048]{1,0:T(8,128)(2,1)S(1)}, u32[]{:S(2)}, u32[]{:S(2)}) collective-permute-start(bf16[16,2048]{1,0:T(8,128)(2,1)S(1)} %get-tuple-element.10), channel_id=1, source_target_pairs={{0,12},{1,13},{2,14},{3,15},{4,8},{5,9},{6,10},{7,11},{8,4},{9,5},... | collective-permute-start | bytes 196616 | tf_op jit(solution)/shard_map/ppermute | solution.py:54
  143.1 7.1 %collective-permute-start.18 = (bf16[16,2048]{1,0:T(8,128)(2,1)S(1)}, bf16[16,2048]{1,0:T(8,128)(2,1)S(1)}, u32[]{:S(2)}, u32[]{:S(2)}) collective-permute-start(bf16[16,2048]{1,0:T(8,128)(2,1)S(1)} %get-tuple-element.10), channel_id=1, source_target_pairs={{0,14},{1,15},{2,12},{3,13},{4,10},{5,11},{6,8},{7,9},{8,6},{9,7},... | collective-permute-start | bytes 196616 | tf_op jit(solution)/shard_map/ppermute | solution.py:54
  161.7 8.2 %collective-permute-start.26 = (bf16[16,2048]{1,0:T(8,128)(2,1)S(1)}, bf16[16,2048]{1,0:T(8,128)(2,1)S(1)}, u32[]{:S(2)}, u32[]{:S(2)}) collective-permute-start(bf16[16,2048]{1,0:T(8,128)(2,1)S(1)} %get-tuple-element.39), channel_id=1, source_target_pairs={{0,4},{1,5},{2,6},{3,7},{4,0},{5,1},{6,2},{7,3},{8,12},{9,13},{10,... | collective-permute-start | bytes 196616 | tf_op jit(solution)/shard_map/ppermute | solution.py:54
  163.4 8.9 %collective-permute-start.27 = (bf16[16,2048]{1,0:T(8,128)(2,1)S(1)}, bf16[16,2048]{1,0:T(8,128)(2,1)S(1)}, u32[]{:S(2)}, u32[]{:S(2)}) collective-permute-start(bf16[16,2048]{1,0:T(8,128)(2,1)S(1)} %get-tuple-element.38), channel_id=1, source_target_pairs={{0,6},{1,7},{2,4},{3,5},{4,2},{5,3},{6,0},{7,1},{8,14},{9,15},{10,... | collective-permute-start | bytes 196616 | tf_op jit(solution)/shard_map/ppermute | solution.py:54
  164.6 9.2 %collective-permute-start.28 = (bf16[16,2048]{1,0:T(8,128)(2,1)S(1)}, bf16[16,2048]{1,0:T(8,128)(2,1)S(1)}, u32[]{:S(2)}, u32[]{:S(2)}) collective-permute-start(bf16[16,2048]{1,0:T(8,128)(2,1)S(1)} %get-tuple-element.37), channel_id=1, source_target_pairs={{0,8},{1,9},{2,10},{3,11},{4,12},{5,13},{6,14},{7,15},{8,0},{9,1},... | collective-permute-start | bytes 196616 | tf_op jit(solution)/shard_map/ppermute | solution.py:54
  166.5 9.5 %collective-permute-start.29 = (bf16[16,2048]{1,0:T(8,128)(2,1)S(1)}, bf16[16,2048]{1,0:T(8,128)(2,1)S(1)}, u32[]{:S(2)}, u32[]{:S(2)}) collective-permute-start(bf16[16,2048]{1,0:T(8,128)(2,1)S(1)} %get-tuple-element.36), channel_id=1, source_target_pairs={{0,10},{1,11},{2,8},{3,9},{4,14},{5,15},{6,12},{7,13},{8,2},{9,3},... | collective-permute-start | bytes 196616 | tf_op jit(solution)/shard_map/ppermute | solution.py:54
  167.5 8.5 %collective-permute-start.30 = (bf16[16,2048]{1,0:T(8,128)(2,1)S(1)}, bf16[16,2048]{1,0:T(8,128)(2,1)S(1)}, u32[]{:S(2)}, u32[]{:S(2)}) collective-permute-start(bf16[16,2048]{1,0:T(8,128)(2,1)S(1)} %get-tuple-element.35), channel_id=1, source_target_pairs={{0,12},{1,13},{2,14},{3,15},{4,8},{5,9},{6,10},{7,11},{8,4},{9,5},... | collective-permute-start | bytes 196616 | tf_op jit(solution)/shard_map/ppermute | solution.py:54
  177.1 8.0 %collective-permute-start.32 = (bf16[16,2048]{1,0:T(8,128)(2,1)S(1)}, bf16[16,2048]{1,0:T(8,128)(2,1)S(1)}, u32[]{:S(2)}, u32[]{:S(2)}) collective-permute-start(bf16[16,2048]{1,0:T(8,128)(2,1)S(1)} %get-tuple-element.8), channel_id=1, source_target_pairs={{0,2},{1,3},{2,0},{3,1},{4,6},{5,7},{6,4},{7,5},{8,10},{9,11},{10,... | collective-permute-start | bytes 196616 | tf_op jit(solution)/shard_map/ppermute | solution.py:54
  178.9 8.6 %collective-permute-start.33 = (bf16[16,2048]{1,0:T(8,128)(2,1)S(1)}, bf16[16,2048]{1,0:T(8,128)(2,1)S(1)}, u32[]{:S(2)}, u32[]{:S(2)}) collective-permute-start(bf16[16,2048]{1,0:T(8,128)(2,1)S(1)} %get-tuple-element.8), channel_id=1, source_target_pairs={{0,4},{1,5},{2,6},{3,7},{4,0},{5,1},{6,2},{7,3},{8,12},{9,13},{10,... | collective-permute-start | bytes 196616 | tf_op jit(solution)/shard_map/ppermute | solution.py:54
  181.2 8.3 %collective-permute-start.34 = (bf16[16,2048]{1,0:T(8,128)(2,1)S(1)}, bf16[16,2048]{1,0:T(8,128)(2,1)S(1)}, u32[]{:S(2)}, u32[]{:S(2)}) collective-permute-start(bf16[16,2048]{1,0:T(8,128)(2,1)S(1)} %get-tuple-element.8), channel_id=1, source_target_pairs={{0,6},{1,7},{2,4},{3,5},{4,2},{5,3},{6,0},{7,1},{8,14},{9,15},{10,... | collective-permute-start | bytes 196616 | tf_op jit(solution)/shard_map/ppermute | solution.py:54
  181.7 10.4 %collective-permute-start.35 = (bf16[16,2048]{1,0:T(8,128)(2,1)S(1)}, bf16[16,2048]{1,0:T(8,128)(2,1)S(1)}, u32[]{:S(2)}, u32[]{:S(2)}) collective-permute-start(bf16[16,2048]{1,0:T(8,128)(2,1)S(1)} %get-tuple-element.8), channel_id=1, source_target_pairs={{0,8},{1,9},{2,10},{3,11},{4,12},{5,13},{6,14},{7,15},{8,0},{9,1},... | collective-permute-start | bytes 196616 | tf_op jit(solution)/shard_map/ppermute | solution.py:54
  184.3 9.5 %collective-permute-start.36 = (bf16[16,2048]{1,0:T(8,128)(2,1)S(1)}, bf16[16,2048]{1,0:T(8,128)(2,1)S(1)}, u32[]{:S(2)}, u32[]{:S(2)}) collective-permute-start(bf16[16,2048]{1,0:T(8,128)(2,1)S(1)} %get-tuple-element.8), channel_id=1, source_target_pairs={{0,10},{1,11},{2,8},{3,9},{4,14},{5,15},{6,12},{7,13},{8,2},{9,3},... | collective-permute-start | bytes 196616 | tf_op jit(solution)/shard_map/ppermute | solution.py:54
  185.1 8.7 %collective-permute-start.37 = (bf16[16,2048]{1,0:T(8,128)(2,1)S(1)}, bf16[16,2048]{1,0:T(8,128)(2,1)S(1)}, u32[]{:S(2)}, u32[]{:S(2)}) collective-permute-start(bf16[16,2048]{1,0:T(8,128)(2,1)S(1)} %get-tuple-element.8), channel_id=1, source_target_pairs={{0,12},{1,13},{2,14},{3,15},{4,8},{5,9},{6,10},{7,11},{8,4},{9,5},... | collective-permute-start | bytes 196616 | tf_op jit(solution)/shard_map/ppermute | solution.py:54
  187.5 7.1 %collective-permute-start.38 = (bf16[16,2048]{1,0:T(8,128)(2,1)S(1)}, bf16[16,2048]{1,0:T(8,128)(2,1)S(1)}, u32[]{:S(2)}, u32[]{:S(2)}) collective-permute-start(bf16[16,2048]{1,0:T(8,128)(2,1)S(1)} %get-tuple-element.8), channel_id=1, source_target_pairs={{0,14},{1,15},{2,12},{3,13},{4,10},{5,11},{6,8},{7,9},{8,6},{9,7},... | collective-permute-start | bytes 196616 | tf_op jit(solution)/shard_map/ppermute | solution.py:54
  (29 other events, 104.3 us)
